TPU v7x, 32 devices: a whole 2x2x4 slice. The times are simulated.
32 devices in a mesh: sp: 16 (over z, y, x), tp: 2 (over core).
Axes of the slice: x: 2, y: 2, z: 4, core: 2. Of those that a mesh axis runs over, the one named last changes fastest.
Arguments:
- stream: bfloat16 [4096, 2048], P(('sp', 'tp')), may hold values from -6 to 6
- outer_gate: bfloat16 [4096, 1024], P('sp', 'tp'), may hold values from -6 to 6
- inner_gate: bfloat16 [4096, 1024], P('sp', 'tp'), may hold values from -6 to 6
- conv_values: bfloat16 [4096, 1024], P('sp', 'tp'), may hold values from -6 to 6
- doc_ids: int32 [4096], P('sp'), may hold values from 0 to 7, never falling along the last dimension, each value on 1 to 1024 neighbouring positions
- conv_taps: float32 [3, 1024], P(None, 'tp'), may hold values from -3.5 to 3.5
- out_weight: bfloat16 [1024, 2048], replicated, may hold values from -0.1875 to 0.1875
- norm_gain: float32 [2048], replicated, may hold values from 0.1 to 1.9
- route_ids: int32 [4096, 2], P(('sp', 'tp')), may hold values from 0 to 31, all different within a row; in each aligned block of 128 rows (0 to 127, 128 to 255, ...) at most 16 rows name the same one
- route_logits: float32 [4096, 2], P(('sp', 'tp')), may hold values from -4 to 4
- group_weight: float32 [4096], P(('sp', 'tp')), may hold values from 0.25 to 1
- w_gate: bfloat16 [32, 2048, 1024], P(('sp', 'tp')), may hold values from -0.125 to 0.125
- w_up: bfloat16 [32, 2048, 1024], P(('sp', 'tp')), may hold values from -0.125 to 0.125
- w_down: bfloat16 [32, 1024, 2048], P(('sp', 'tp')), may hold values from -0.1875 to 0.1875
Outputs:
- result: bfloat16 [4096, 2048], P(('sp', 'tp'))
Inputs may be any that keep to these rules, and one draw needn't show every extreme that they name: `route_ids`: the two experts of a token differ. In the rows of one device (aligned blocks of 128 rows) no expert is named more than 16 times, a bound that some block reaches. `doc_ids`: document numbers never fall along the sequence; a document has 1 to 1024 positions and one has exactly 1024.
All inputs are finite; a program needn't handle non-finite values.
Results may differ from a plain program's by a relative error of at most 0.0052.
Values may be sent and summed in bfloat16 or wider, within the bound.
A program may use at most 64 MiB of HBM per device.

v0:
```python
import jax
import jax.numpy as jnp
from jax import lax
from jax.sharding import PartitionSpec as P


def padded_2(shard, sides, width):
    for axis, dim in sides:
        size, length = (lax.axis_size(axis), shard.shape[dim])
        up = [(i, (i + 1) % size) for i in range(size - 1)]
        down = [(j, i) for i, j in up]
        last = lax.slice_in_dim(shard, length - width, length, axis=dim)
        leading = lax.slice_in_dim(shard, 0, width, axis=dim)
        before = lax.ppermute(last, axis, up)
        after = lax.ppermute(leading, axis, down)
        shard = jnp.concatenate([before, shard, after], axis=dim)
    return shard


def on_device(
    stream,
    outer_gate,
    inner_gate,
    conv_values,
    doc_ids,
    conv_taps,
    out_weight,
    norm_gain,
    route_ids,
    route_logits,
    group_weight,
    w_gate,
    w_up,
    w_down,
):
    tok_rows = stream.shape[0]
    width = stream.shape[1]
    product = (inner_gate.astype(jnp.float32) * conv_values.astype(jnp.float32)).astype(
        jnp.bfloat16
    )
    doc_float = doc_ids.astype(jnp.bfloat16)
    padded, padded_docs = (padded_2(product, (("sp", 0),), 1), padded_2(doc_float, (("sp", 0),), 1))
    same_prev = (padded_docs[:-2] == doc_float).astype(jnp.float32)[:, None]
    same_next = (padded_docs[2:] == doc_float).astype(jnp.float32)[:, None]
    conv = (
        conv_taps[0] * padded[:-2].astype(jnp.float32) * same_prev
        + conv_taps[1] * product.astype(jnp.float32)
        + conv_taps[2] * padded[2:].astype(jnp.float32) * same_next
    )
    mixed = (outer_gate.astype(jnp.float32) * conv).astype(jnp.bfloat16)
    channels = lax.all_to_all(mixed, "tp", split_axis=0, concat_axis=1, tiled=True)
    projected = jnp.dot(channels, out_weight, preferred_element_type=jnp.float32)
    resid = stream.astype(jnp.float32) + projected
    scale = lax.rsqrt(jnp.mean(resid * resid, axis=-1, keepdims=True) + 1e-06)
    normed = (resid * scale * norm_gain).astype(jnp.bfloat16)
    expert_total = lax.axis_size("sp") * lax.axis_size("tp")
    top_count = route_ids.shape[1]
    capacity = 2 * tok_rows * top_count // expert_total
    flat_ids = route_ids.reshape(-1)
    one_hot = (flat_ids[:, None] == jnp.arange(expert_total, dtype=jnp.int32)[None, :]).astype(
        jnp.int32
    )
    rank = jnp.sum((jnp.cumsum(one_hot, axis=0) - 1) * one_hot, axis=1)
    slot = flat_ids * capacity + rank
    slot_count = expert_total * capacity
    source_row = (
        jnp.zeros((slot_count,), jnp.int32)
        .at[slot]
        .set(jnp.arange(flat_ids.shape[0], dtype=jnp.int32) // top_count)
    )
    filled = jnp.zeros((slot_count,), jnp.bool_).at[slot].set(True)
    outgoing = jnp.where(filled[:, None], normed[source_row], jnp.zeros((), jnp.bfloat16)).reshape(
        expert_total, capacity, width
    )
    arrived = lax.all_to_all(outgoing, ("sp", "tp"), split_axis=0, concat_axis=0, tiled=True)
    sources, items, features = arrived.shape
    rows_in = arrived.reshape(sources * items, features)
    hidden = (
        jax.nn.silu(jnp.dot(rows_in, w_gate[0], preferred_element_type=jnp.float32))
        * jnp.dot(rows_in, w_up[0], preferred_element_type=jnp.float32)
    ).astype(jnp.bfloat16)
    outputs = jnp.dot(hidden, w_down[0], preferred_element_type=jnp.float32).astype(jnp.bfloat16)
    returned = lax.all_to_all(
        outputs.reshape(sources, items, features),
        ("sp", "tp"),
        split_axis=0,
        concat_axis=0,
        tiled=True,
    )
    picked = (
        returned.reshape(slot_count, width)[slot]
        .astype(jnp.float32)
        .reshape(tok_rows, top_count, width)
    )
    expo = jnp.exp(route_logits)
    gate = group_weight[:, None] * expo / jnp.sum(expo, axis=1, keepdims=True)
    result = resid + jnp.sum(gate[:, :, None] * picked, axis=1)
    return result.astype(jnp.bfloat16)


def solution(mesh):
    placed = (
        P(("sp", "tp"), None),
        P("sp", "tp"),
        P("sp", "tp"),
        P("sp", "tp"),
        P("sp"),
        P(None, "tp"),
        P(),
        P(),
        P(("sp", "tp"), None),
        P(("sp", "tp"), None),
        P(("sp", "tp")),
        P(("sp", "tp"), None, None),
        P(("sp", "tp"), None, None),
        P(("sp", "tp"), None, None),
    )
    return jax.shard_map(
        on_device, mesh=mesh, in_specs=placed, out_specs=P(("sp", "tp"), None), check_vma=False
    )
```

profile of v0, /device:TPU:0, one launch (start us, length us, event | category | flops | bytes accessed | tf_op | source)
XLA Modules:
  0.0 169.3 jit_solution(4151391438809360174)
XLA Ops:
  0.0 0.7 convert_element_type.66
  0.7 0.6 fusion.23
  1.3 5.4 %collective-permute-start.1 = (bf16[1]{0:T(256)(128)(2,1)}, bf16[1]{0:T(256)(128)(2,1)}, u32[]{:S(2)}, u32[]{:S(2)}) collective-permute-start(bf16[1]{0:T(256)(128)(2,1)} %get-tuple-element.14), channel_id=1, source_target_pairs={{0,2},{2,4},{4,6},{6,8},{8,10},{10,12},{12,14},{14,16},{16,18},{18... | collective-permute-start | bytes 14 | tf_op jit(solution)/shard_map/ppermute | solution.py:14
  6.7 1.3 collective-permute-start.3
  8.0 1.1 multiply_convert_fusion.3
  9.1 4.5 %collective-permute-start = (bf16[1,512]{1,0:T(2,128)(2,1)S(1)}, bf16[1,512]{1,0:T(2,128)(2,1)S(1)}, u32[]{:S(2)}, u32[]{:S(2)}) collective-permute-start(bf16[1,512]{1,0:T(2,128)(2,1)S(1)} %get-tuple-element.5), channel_id=1, source_target_pairs={{0,2},{2,4},{4,6},{6,8},{8,10},{10,12},{12,14},{14,16},{16,18},{18... | collective-permute-start | bytes 3080 | tf_op jit(solution)/shard_map/ppermute | solution.py:14
  13.7 1.3 collective-permute-start.2
  15.0 0.8 copy.24
  16.0 0.7 broadcast_multiply_fusion
  16.7 0.8 fusion.22
  17.5 0.6 reduce-window.6
  18.1 0.2 slice_reduce_fusion
  18.7 1.4 scatter_custom_fusion.1
  20.2 1.5 scatter_custom_fusion
  21.8 1.3 pad_maximum_fusion.2
  23.0 0.8 compare_convert_fusion.1
  23.8 1.2 multiply_convert_fusion.2
  25.0 3.9 %all_to_all.29 = bf16[2,128,512]{2,1,0:T(8,128)(2,1)S(1)} all-to-all(bf16[2,128,512]{2,1,0:T(8,128)(2,1)S(1)} %bitcast.51), channel_id=1, replica_groups=mesh['sp'=16,'tp'=2] {'tp'}, dimensions={0} | all-to-all | bytes 524288 | tf_op jit(solution)/shard_map/all_to_all | solution.py:51
  29.0 0.2 copy.21
  29.2 3.0 %multiply_reduce_fusion.1 = (f32[128]{0:T(128)S(1)}, f32[128,2048]{1,0:T(8,128)S(1)}) fusion(bf16[128,1024]{0,1:T(8,128)(2,1)S(1)} %bitcast.52, bf16[1024,2048]{1,0:T(8,128)(2,1)} %param.20, bf16[128,2048]{1,0:T(8,128)(2,1)S(1)} %copy-done), kind=kOutput, calls=%fused_computation.17 | convolution fusion | flops 537919360 | bytes 6029824 | tf_op jit(solution)/shard_map/dot_general | solution.py:52
  32.2 0.2 multiply_convert_fusion.1
  32.4 3.3 %gather_fusion = bf16[512,2048]{1,0:T(8,128)(2,1)} fusion(bf16[128,2048]{1,0:T(8,128)(2,1)S(1)} %multiply_convert_fusion.1, s32[1024]{0:T(1024)S(1)} %pad_clamp_fusion.1), kind=kCustom, calls=%fused_computation | custom fusion | bytes 4196352 | tf_op jit(solution)/shard_map/gather | solution.py:72
  35.7 1.8 %broadcast_select_fusion = bf16[32,16,2048]{2,1,0:T(8,128)(2,1)S(1)} fusion(bf16[32,16,2048]{2,1,0:T(8,128)(2,1)} %bitcast.47, pred[32,16]{1,0:T(8,128)(4,1)S(1)} %broadcast_in_dim.22), kind=kLoop, calls=%fused_computation.14 | loop fusion | flops 1048576 | bytes 4194816 | tf_op jit(solution)/shard_map/jit(_where)/select_n | solution.py:72
  37.5 56.7 %all_to_all.30 = bf16[32,16,2048]{2,1,0:T(8,128)(2,1)S(1)} all-to-all(bf16[32,16,2048]{2,1,0:T(8,128)(2,1)S(1)} %broadcast_select_fusion), channel_id=1, replica_groups=mesh['sp'=16,'tp'=2] {'sp','tp'}, dimensions={0} | all-to-all | bytes 4194304 | tf_op jit(solution)/shard_map/all_to_all | solution.py:75
  94.3 3.7 %fusion.4 = f32[512,1024]{1,0:T(8,128)} fusion(bf16[512,2048]{1,0:T(8,128)(2,1)S(1)} %bitcast.49, bf16[1,2048,1024]{2,1,0:T(8,128)(2,1)S(1)} %copy-done.4), kind=kOutput, calls=%fused_computation.8 | convolution fusion | flops 2147483648 | bytes 8388608 | tf_op jit(solution)/shard_map/dot_general | solution.py:79
  98.0 9.9 %fusion.6 = bf16[512,2048]{1,0:T(8,128)(2,1)} fusion(bf16[1,1024,2048]{2,1,0:T(8,128)(2,1)} %param.27, f32[512,1024]{1,0:T(8,128)} %fusion.4, bf16[512,2048]{1,0:T(8,128)(2,1)S(1)} %bitcast.50, bf16[1,2048,1024]{2,1,0:T(8,128)(2,1)} %param.26), kind=kOutput, calls=%fused_computation.10 | convolution fusion | flops 4299161600 | bytes 14680064 | tf_op jit(solution)/shard_map/dot_general | solution.py:82
  107.9 3.8 %all-to-all-start.2 = ((bf16[32,16,2048]{2,1,0:T(8,128)(2,1)}), bf16[32,16,2048]{2,1,0:T(8,128)(2,1)S(1)}, u32[]{:S(2)}, u32[]{:S(2)}) async-start(bf16[32,16,2048]{2,1,0:T(8,128)(2,1)} %bitcast.48), calls=%async_computation.2 | async-start | bytes 4194304 | tf_op jit(solution)/shard_map/all_to_all | solution.py:83
  111.9 48.5 %all-to-all-done.2 = bf16[32,16,2048]{2,1,0:T(8,128)(2,1)S(1)} async-done(((bf16[32,16,2048]{2,1,0:T(8,128)(2,1)}), bf16[32,16,2048]{2,1,0:T(8,128)(2,1)S(1)}, u32[]{:S(2)}, u32[]{:S(2)}) %all-to-all-start.2) | async-done | bytes 2097184 | tf_op jit(solution)/shard_map/all_to_all | solution.py:83
  160.4 2.3 %gather_fusion.1 = bf16[256,2048]{1,0:T(8,128)(2,1)} fusion(bf16[512,2048]{1,0:T(8,128)(2,1)S(1)} %bitcast.46, s32[1024]{0:T(1024)S(1)} %pad_clamp_fusion), kind=kCustom, calls=%fused_computation.1 | custom fusion | bytes 2098176 | tf_op jit(solution)/shard_map/gather | solution.py:91
  162.8 2.4 %reshape.90 = f32[128,2,2048]{2,1,0:T(2,128)S(1)} reshape(bf16[256,2048]{1,0:T(8,128)(2,1)} %gather_fusion.1) | data formatting | bytes 3145728 | tf_op jit(solution)/shard_map/convert_element_type | solution.py:92
  165.1 3.2 %multiply_reduce_fusion = f32[128,2048]{1,0:T(8,128)S(1)} fusion(f32[128,2,2048]{2,1,0:T(2,128)S(1)} %reshape.90, f32[128,2]{1,0:T(8,128)S(1)} %copy.22), kind=kLoop, calls=%fused_computation.12 | loop fusion | flops 786432 | bytes 3146752 | tf_op jit(solution)/shard_map/reduce_sum | solution.py:97
  168.3 0.9 add_convert_fusion
  (34 shorter events, 1.0 us)
Async XLA Ops:
  0.0 29.2 %copy-start = (bf16[128,2048]{1,0:T(8,128)(2,1)S(1)}, bf16[128,2048]{1,0:T(8,128)(2,1)}, u32[]{:S(2)}) copy-start(bf16[128,2048]{1,0:T(8,128)(2,1)} %param.14) | copy-start | bytes 1572868
  1.3 20.4 %collective-permute-start.1 = (bf16[1]{0:T(256)(128)(2,1)}, bf16[1]{0:T(256)(128)(2,1)}, u32[]{:S(2)}, u32[]{:S(2)}) collective-permute-start(bf16[1]{0:T(256)(128)(2,1)} %get-tuple-element.14), channel_id=1, source_target_pairs={{0,2},{2,4},{4,6},{6,8},{8,10},{10,12},{12,14},{14,16},{16,18},{18... | collective-permute-start | bytes 14 | tf_op jit(solution)/shard_map/ppermute | solution.py:14
  6.7 15.1 %collective-permute-start.3 = (bf16[1]{0:T(256)(128)(2,1)}, bf16[1]{0:T(256)(128)(2,1)}, u32[]{:S(2)}, u32[]{:S(2)}) collective-permute-start(bf16[1]{0:T(256)(128)(2,1)} %get-tuple-element.15), channel_id=1, source_target_pairs={{2,0},{4,2},{6,4},{8,6},{10,8},{12,10},{14,12},{16,14},{18,16},{20... | collective-permute-start | bytes 14 | tf_op jit(solution)/shard_map/ppermute | solution.py:15
  9.1 14.7 %collective-permute-start = (bf16[1,512]{1,0:T(2,128)(2,1)S(1)}, bf16[1,512]{1,0:T(2,128)(2,1)S(1)}, u32[]{:S(2)}, u32[]{:S(2)}) collective-permute-start(bf16[1,512]{1,0:T(2,128)(2,1)S(1)} %get-tuple-element.5), channel_id=1, source_target_pairs={{0,2},{2,4},{4,6},{6,8},{8,10},{10,12},{12,14},{14,16},{16,18},{18... | collective-permute-start | bytes 3080 | tf_op jit(solution)/shard_map/ppermute | solution.py:14
  13.7 10.1 %collective-permute-start.2 = (bf16[1,512]{1,0:T(2,128)(2,1)S(1)}, bf16[1,512]{1,0:T(2,128)(2,1)S(1)}, u32[]{:S(2)}, u32[]{:S(2)}) collective-permute-start(bf16[1,512]{1,0:T(2,128)(2,1)S(1)} %get-tuple-element.6), channel_id=1, source_target_pairs={{2,0},{4,2},{6,4},{8,6},{10,8},{12,10},{14,12},{16,14},{18,16},{20... | collective-permute-start | bytes 3080 | tf_op jit(solution)/shard_map/ppermute | solution.py:15
  29.2 3.0 %copy-start.1 = (f32[2048]{0:T(1024)S(1)}, f32[2048]{0:T(1024)}, u32[]{:S(2)}) copy-start(f32[2048]{0:T(1024)} %param.21) | copy-start | bytes 24580
  37.5 56.7 %copy-start.4 = (bf16[1,2048,1024]{2,1,0:T(8,128)(2,1)S(1)}, bf16[1,2048,1024]{2,1,0:T(8,128)(2,1)}, u32[]{:S(2)}) copy-start(bf16[1,2048,1024]{2,1,0:T(8,128)(2,1)} %param.25) | copy-start | bytes 12582916
  107.9 3.8 %copy-start.2 = (f32[128,2]{0,1:T(2,128)S(1)}, f32[128,2]{0,1:T(2,128)}, u32[]{:S(2)}) copy-start(f32[128,2]{0,1:T(2,128)} %param.23) | copy-start | bytes 3076
  107.9 3.9 %copy-start.3 = (f32[128]{0:T(128)S(1)}, f32[128]{0:T(128)}, u32[]{:S(2)}) copy-start(f32[128]{0:T(128)} %param.24) | copy-start | bytes 1540
  107.9 52.5 %all-to-all-start.2 = ((bf16[32,16,2048]{2,1,0:T(8,128)(2,1)}), bf16[32,16,2048]{2,1,0:T(8,128)(2,1)S(1)}, u32[]{:S(2)}, u32[]{:S(2)}) async-start(bf16[32,16,2048]{2,1,0:T(8,128)(2,1)} %bitcast.48), calls=%async_computation.2 | async-start | bytes 4194304 | tf_op jit(solution)/shard_map/all_to_all | solution.py:83
where the time goes:
time: 170 us; the launch traced here: 169 us
  blocking collectives  60.7 us (36%)
  waiting for transfers between devices  48.5 us (29%)
  matrix products  16.6 us (10%)
  starting transfers between devices  16.3 us (10%)
  local copies, waits for them, and re-layouts  14.3 us (8%)
  other arithmetic  12.6 us (7%)
    all_to_all x1, blocking collectives, on_device(): lax.all_to_all(outgoing, ('sp', 'tp'), split_axis=0, concat_axis=0, tiled...  56.7 us
    all_to_all x1, waiting for transfers between devices, on_device(): lax.all_to_all(outputs.reshape(sources, items, features), ('sp', 'tp'), s...  48.5 us
    ppermute x2, starting transfers between devices, padded_2(): before = lax.ppermute(last, axis, up)  9.91 us
    dot_general x1, matrix products, on_device(): jnp.dot(hidden, w_down[0], preferred_element_type=jnp.float32)  9.9 us
    all_to_all x1, blocking collectives, on_device(): lax.all_to_all(mixed, 'tp', split_axis=0, concat_axis=1, tiled=True)  3.94 us
    all_to_all x1, starting transfers between devices, on_device(): lax.all_to_all(outputs.reshape(sources, items, features), ('sp', 'tp'), s...  3.83 us
    dot_general x1, matrix products, on_device(): jnp.dot(rows_in, w_gate[0], preferred_element_type=jnp.float32)  3.73 us
  transfers between devices with their start and end apart: 5, of which 1 were waited for; matrix products, arithmetic and copies ran while one was open for 6% of the time, Pallas kernels for 0%

commit v1 on v0

--- a/solution.py
+++ b/solution.py
@@ -1,6 +1,10 @@
+import functools
+
 import jax
 import jax.numpy as jnp
 from jax import lax
+from jax.experimental import pallas as pl
+from jax.experimental.pallas import tpu as pltpu
 from jax.sharding import PartitionSpec as P
 
 
@@ -98,6 +102,330 @@
     return result.astype(jnp.bfloat16)
 
 
+MESH = pl.DeviceIdType.MESH
+F32, BF16 = jnp.float32, jnp.bfloat16
+
+
+def dot(a, b):
+    return jnp.dot(a, b, preferred_element_type=F32)
+
+
+def flip(z, g):
+    return 2 * ((z // 2 + g // 2) % 2) + (z % 2 + g % 2) % 2
+
+
+def fused_kernel(
+    tp_size, planes, per_plane, cap,
+    stream, outer, inner, values, docs, taps, gain, ids, logits, weight,
+    ow_hbm, wg_hbm, wu_hbm, wd_hbm,
+    out,
+    ow, wg, wu, wd, edge_out, edge_in, doc_in, mix, mix_in, resid, normed, hidden,
+    send, recv, outb, ret,
+    load_sem, edge_send, edge_recv, mix_send, mix_recv, self_sem,
+    out_sem, in_sem, back_sem, home_sem,
+):
+    sp, tp = lax.axis_index("sp"), lax.axis_index("tp")
+    sp_size = planes * per_plane // tp_size
+    total = planes * per_plane
+    me = sp * tp_size + tp
+    z, p = me // per_plane, me % per_plane
+    rows, width = stream.shape
+    chan = inner.shape[1]
+    length = inner.shape[0]
+
+    def place(index):
+        return (index // tp_size, index % tp_size)
+
+    loads = [
+        pltpu.make_async_copy(src, dst, load_sem.at[i])
+        for i, (src, dst) in enumerate(
+            ((ow_hbm, ow), (wg_hbm.at[0], wg), (wu_hbm.at[0], wu), (wd_hbm.at[0], wd))
+        )
+    ]
+    for load in loads:
+        load.start()
+
+    barrier = pltpu.get_barrier_semaphore()
+
+    def greet(i, carry):
+        pl.semaphore_signal(
+            barrier, inc=1, device_id=place((me + i) % total), device_id_type=MESH
+        )
+        return carry
+
+    lax.fori_loop(1, total, greet, 0)
+    product = (inner[...].astype(F32) * values[...].astype(F32)).astype(BF16)
+    edge_out[0] = product[:16]
+    edge_out[1] = product[length - 16 :]
+    pl.semaphore_wait(barrier, total - 1)
+
+    left, right = ((sp + sp_size - 1) % sp_size, tp), ((sp + 1) % sp_size, tp)
+    edges = []
+    for side, (dest, src) in enumerate(((right, edge_out.at[1]), (left, edge_out.at[0]))):
+        for kind, (source, target) in enumerate(
+            ((src, edge_in.at[side]), (docs, doc_in.at[side]))
+        ):
+            edges.append(
+                pltpu.make_async_remote_copy(
+                    src_ref=source,
+                    dst_ref=target,
+                    send_sem=edge_send.at[2 * side + kind],
+                    recv_sem=edge_recv.at[2 * side + kind],
+                    device_id=dest,
+                    device_id_type=MESH,
+                )
+            )
+    for edge in edges:
+        edge.start()
+
+    logit = logits[...]
+    top = logit.shape[0]
+    expo = jnp.exp(logit)
+    gates = weight[...] * expo / jnp.sum(expo, axis=0, keepdims=True)
+    gate_cols = [
+        jnp.transpose(jnp.broadcast_to(gates[k : k + 1], (rows, rows)))[:, :1]
+        for k in range(top)
+    ]
+    before = (
+        lax.broadcasted_iota(jnp.int32, (rows, rows), 0)
+        < lax.broadcasted_iota(jnp.int32, (rows, rows), 1)
+    ).astype(F32).astype(BF16)
+    id_rows = [ids[k : k + 1, :] for k in range(top)]
+    rank_of = lax.broadcasted_iota(jnp.int32, (per_plane, cap, rows), 1).astype(F32)
+
+    def slots(plane):
+        expert = lax.broadcasted_iota(jnp.int32, (per_plane, rows), 0) + plane * per_plane
+        hits = [(row == expert).astype(F32) for row in id_rows]
+        named = sum(hits)
+        ahead = dot(named.astype(BF16), before)
+
+        def spread(hit):
+            at = jnp.where(hit > 0, ahead, -1.0)
+            grid = jnp.broadcast_to(at[:, None, :], (per_plane, cap, rows))
+            return jnp.where(grid == rank_of, 1.0, 0.0).reshape(per_plane * cap, rows)
+
+        return named, hits, spread
+
+    for edge in edges:
+        edge.wait()
+
+    doc = jnp.broadcast_to(docs[...], (8, length))
+    lane = lax.broadcasted_iota(jnp.int32, (8, length), 1)
+    prior = jnp.where(
+        lane == 0,
+        pltpu.roll(jnp.broadcast_to(doc_in[0], (8, length)), 1, axis=1),
+        pltpu.roll(doc, 1, axis=1),
+    )
+    later = jnp.where(
+        lane == length - 1,
+        pltpu.roll(jnp.broadcast_to(doc_in[1], (8, length)), length - 1, axis=1),
+        pltpu.roll(doc, length - 1, axis=1),
+    )
+    spot = lane + sp * length
+    same_prev = jnp.where((prior == doc) & (spot > 0), 1.0, 0.0)
+    same_next = jnp.where((later == doc) & (spot < sp_size * length - 1), 1.0, 0.0)
+
+    def column(row):
+        return jnp.transpose(jnp.broadcast_to(row[:1], (128, length)))[:, :1]
+
+    prod = product.astype(F32)
+    row_at = lax.broadcasted_iota(jnp.int32, (length, chan), 0)
+    prev = jnp.where(row_at == 0, edge_in[0].astype(F32)[15:16], pltpu.roll(prod, 1, axis=0))
+    nxt = jnp.where(
+        row_at == length - 1,
+        edge_in[1].astype(F32)[:1],
+        pltpu.roll(prod, length - 1, axis=0),
+    )
+    conv = (
+        taps[0:1] * prev * column(same_prev)
+        + taps[1:2] * prod
+        + taps[2:3] * nxt * column(same_next)
+    )
+    mixed = (outer[...].astype(F32) * conv).astype(BF16)
+    mix[...] = mixed.reshape(tp_size, rows, chan)
+    other = 1 - tp
+    swap = pltpu.make_async_remote_copy(
+        src_ref=mix.at[other],
+        dst_ref=mix_in,
+        send_sem=mix_send,
+        recv_sem=mix_recv,
+        device_id=(sp, other),
+        device_id_type=MESH,
+    )
+    swap.start()
+    loads[0].wait()
+    tile = 512
+    own = mix[tp]
+    for c in range(0, width, tile):
+        resid[:, c : c + tile] = stream[:, c : c + tile].astype(F32) + dot(
+            own, ow[pl.ds(pl.multiple_of(tp * chan, chan), chan), c : c + tile]
+        )
+    swap.wait()
+    theirs = mix_in[...]
+    squares = jnp.zeros((rows, 1), F32)
+    for c in range(0, width, tile):
+        part = resid[:, c : c + tile] + dot(
+            theirs, ow[pl.ds(pl.multiple_of(other * chan, chan), chan), c : c + tile]
+        )
+        resid[:, c : c + tile] = part
+        squares = squares + jnp.sum(part * part, axis=1, keepdims=True)
+    scale = lax.rsqrt(squares / width + 1e-06)
+    for c in range(0, width, tile):
+        normed[:, c : c + tile] = (
+            resid[:, c : c + tile] * scale * gain[:, c : c + tile]
+        ).astype(BF16)
+
+    def group_copy(src, dst, g, i, source_sem, target_sem):
+        peer = (p + i) % per_plane
+        return pltpu.make_async_remote_copy(
+            src_ref=src.at[g, peer],
+            dst_ref=dst.at[g, p],
+            send_sem=source_sem.at[g],
+            recv_sem=target_sem.at[g],
+            device_id=place(flip(z, g) * per_plane + peer),
+            device_id_type=MESH,
+        )
+
+    def start_group(src, dst, g, source_sem, target_sem):
+        def one(i, carry):
+            @pl.when(g * per_plane + i > 0)
+            def _():
+                group_copy(src, dst, g, i, source_sem, target_sem).start()
+
+            return carry
+
+        lax.fori_loop(0, per_plane, one, 0)
+
+    def wait_group(buf, g, sem):
+        @pl.when(g == 0)
+        def _():
+            part = buf.at[0, pl.ds(0, per_plane - 1)]
+            pltpu.make_async_copy(part, part, sem.at[0]).wait()
+
+        @pl.when(g > 0)
+        def _():
+            pltpu.make_async_copy(buf.at[g], buf.at[g], sem.at[g]).wait()
+
+    def dispatch(n, carry):
+        g = planes - 1 - n
+        named, hits, spread = slots(flip(z, g))
+        pick = spread(named).astype(BF16)
+        for c in range(0, width, tile):
+            send[g, :, :, c : c + tile] = (
+                dot(pick, normed[:, c : c + tile])
+                .astype(BF16)
+                .reshape(per_plane, cap, tile)
+            )
+        start_group(send, recv, g, out_sem, in_sem)
+        return carry
+
+    lax.fori_loop(0, planes, dispatch, 0)
+    keep = pltpu.make_async_copy(send.at[0, p], recv.at[0, p], self_sem)
+    keep.start()
+    keep.wait()
+    for load in loads[1:]:
+        load.wait()
+
+    def experts(g, carry):
+        wait_group(recv, g, in_sem)
+        x = recv[g].reshape(per_plane * cap, width)
+        ff = hidden.shape[1]
+        for f in range(0, ff, 256):
+            a = dot(x, wg[:, f : f + 256])
+            b = dot(x, wu[:, f : f + 256])
+            hidden[:, f : f + 256] = (a / (1.0 + jnp.exp(-a)) * b).astype(BF16)
+        h = hidden[...]
+        for c in range(0, width, tile):
+            outb[g, :, :, c : c + tile] = (
+                dot(h, wd[:, c : c + tile]).astype(BF16).reshape(per_plane, cap, tile)
+            )
+        start_group(outb, ret, g, back_sem, home_sem)
+        return carry
+
+    lax.fori_loop(0, planes, experts, 0)
+    keep_back = pltpu.make_async_copy(outb.at[0, p], ret.at[0, p], self_sem)
+    keep_back.start()
+    keep_back.wait()
+
+    def combine(g, carry):
+        wait_group(ret, g, home_sem)
+        named, hits, spread = slots(flip(z, g))
+        picks = [jnp.transpose(spread(hit)).astype(BF16) for hit in hits]
+        for c in range(0, width, tile):
+            rows_in = ret[g, :, :, c : c + tile].reshape(per_plane * cap, tile)
+            resid[:, c : c + tile] += sum(
+                gate * dot(pick, rows_in) for gate, pick in zip(gate_cols, picks)
+            )
+        return carry
+
+    lax.fori_loop(0, planes, combine, 0)
+    out[...] = resid[...].astype(BF16)
+
+    def drain(g, carry):
+        wait_group(send, g, out_sem)
+        wait_group(outb, g, back_sem)
+        return carry
+
+    lax.fori_loop(0, planes, drain, 0)
+
+
+def fused(
+    tp_size, planes, per_plane, cap,
+    stream, outer_gate, inner_gate, conv_values, doc_ids, conv_taps, out_weight, norm_gain,
+    route_ids, route_logits, group_weight, w_gate, w_up, w_down,
+):
+    rows, width = stream.shape
+    length, chan = inner_gate.shape
+    ff = w_gate.shape[2]
+    top = route_ids.shape[1]
+    vmem = pl.BlockSpec(memory_space=pltpu.VMEM)
+    anywhere = pl.BlockSpec(memory_space=pl.ANY)
+    blocks = pltpu.VMEM((planes, per_plane, cap, width), BF16)
+    dma = pltpu.SemaphoreType.DMA
+    return pl.pallas_call(
+        functools.partial(fused_kernel, tp_size, planes, per_plane, cap),
+        out_shape=jax.ShapeDtypeStruct((rows, width), BF16),
+        in_specs=[vmem] * 10 + [anywhere] * 4,
+        out_specs=vmem,
+        scratch_shapes=[
+            pltpu.VMEM(out_weight.shape, BF16),
+            pltpu.VMEM((width, ff), BF16),
+            pltpu.VMEM((width, ff), BF16),
+            pltpu.VMEM((ff, width), BF16),
+            pltpu.VMEM((2, 16, chan), BF16),
+            pltpu.VMEM((2, 16, chan), BF16),
+            pltpu.VMEM((2, 1, length), jnp.int32),
+            pltpu.VMEM((tp_size, rows, chan), BF16),
+            pltpu.VMEM((rows, chan), BF16),
+            pltpu.VMEM((rows, width), F32),
+            pltpu.VMEM((rows, width), BF16),
+            pltpu.VMEM((per_plane * cap, ff), BF16),
+            blocks, blocks, blocks, blocks,
+            dma((4,)), dma((4,)), dma((4,)), dma, dma, dma,
+            dma((planes,)), dma((planes,)), dma((planes,)), dma((planes,)),
+        ],
+        compiler_params=pltpu.CompilerParams(
+            collective_id=0, has_side_effects=True, vmem_limit_bytes=56 * 1024 * 1024
+        ),
+    )(
+        stream, outer_gate, inner_gate, conv_values, doc_ids[None, :], conv_taps,
+        norm_gain[None, :], route_ids.T, route_logits.T, group_weight[None, :],
+        out_weight, w_gate, w_up, w_down,
+    )
+
+
+def body(*args):
+    stream, route_ids = args[0], args[8]
+    tp_size = lax.axis_size("tp")
+    total = lax.axis_size("sp") * tp_size
+    cap = 2 * stream.shape[0] * route_ids.shape[1] // total
+    planes = 4
+    per_plane = total // planes
+    if tp_size != 2 or total % planes or cap % 16 or per_plane * cap != stream.shape[0]:
+        return on_device(*args)
+    return fused(tp_size, planes, per_plane, cap, *args)
+
+
 def solution(mesh):
     placed = (
         P(("sp", "tp"), None),
@@ -116,5 +444,5 @@
         P(("sp", "tp"), None, None),
     )
     return jax.shard_map(
-        on_device, mesh=mesh, in_specs=placed, out_specs=P(("sp", "tp"), None), check_vma=False
-    )
+        body, mesh=mesh, in_specs=placed, out_specs=P(("sp", "tp"), None), check_vma=False
+    )

time: 170 us -> 111 us (0.65)
  the two profiles are of different devices: /device:TPU:0 before, /device:TPU:19 now
where the time goes in v1:
time: 111 us; the launch traced here: 110 us
  Pallas kernels  109 us (98%)
  local copies, waits for them, and re-layouts  1.88 us (2%)
    pallas_call x1, Pallas kernels, fused(): pl.pallas_call(functools.partial(fused_kernel, tp_size, planes, per_plane...  109 us

profile of v1, /device:TPU:19, one launch (start us, length us, event | category | flops | bytes accessed | tf_op | source)
XLA Modules:
  0.0 110.4 jit_solution(1692277031724089447)
XLA Ops:
  0.0 108.6 %shard_map.136 = bf16[128,2048]{1,0:T(8,128)(2,1)} custom-call(bf16[128,2048]{1,0:T(8,128)(2,1)} %stream.1, bf16[256,512]{1,0:T(8,128)(2,1)} %outer.1, bf16[256,512]{1,0:T(8,128)(2,1)} %inner.1, bf16[256,512]{1,0:T(8,128)(2,1)} %values.1, s32[1,256]{1,0:T(1,128)} %bitcast.6, f32[3,512]{1,0:T(4,128)} %taps.1, f32[1,2048]{1,0:T(1,128)} %bitcast.5, ...), custom_call_target="tpu_custom_call" | custom-call | tf_op jit(solution)/shard_map/pallas_call | solution.py:385
  108.6 1.9 %copy.16 = bf16[128,2048]{1,0:T(8,128)(2,1)} copy(bf16[128,2048]{1,0:T(8,128)(2,1)} %shard_map.136) | data formatting | bytes 1048576

commit v2 on v1

--- a/solution.py
+++ b/solution.py
@@ -110,8 +110,15 @@
     return jnp.dot(a, b, preferred_element_type=F32)
 
 
-def flip(z, g):
-    return 2 * ((z // 2 + g // 2) % 2) + (z % 2 + g % 2) % 2
+PARTS = 4
+
+
+def near(z, h):
+    return 2 * (z // 2) + (z % 2 + h) % 2
+
+
+def across(z):
+    return 2 * ((z // 2 + 1) % 2) + z % 2
 
 
 def fused_kernel(
@@ -120,9 +127,9 @@
     ow_hbm, wg_hbm, wu_hbm, wd_hbm,
     out,
     ow, wg, wu, wd, edge_out, edge_in, doc_in, mix, mix_in, resid, normed, hidden,
-    send, recv, outb, ret,
-    load_sem, edge_send, edge_recv, mix_send, mix_recv, self_sem,
-    out_sem, in_sem, back_sem, home_sem,
+    send, recv, outb, ret, far, far_ids, far_logits, far_weight, halves, part_in,
+    load_sem, edge_send, edge_recv, mix_send, mix_recv, self_sem, self_back,
+    out_sem, in_sem, back_sem, home_sem, far_send, far_recv, part_send, part_recv,
 ):
     sp, tp = lax.axis_index("sp"), lax.axis_index("tp")
     sp_size = planes * per_plane // tp_size
@@ -178,22 +185,45 @@
     for edge in edges:
         edge.start()
 
-    logit = logits[...]
-    top = logit.shape[0]
-    expo = jnp.exp(logit)
-    gates = weight[...] * expo / jnp.sum(expo, axis=0, keepdims=True)
-    gate_cols = [
-        jnp.transpose(jnp.broadcast_to(gates[k : k + 1], (rows, rows)))[:, :1]
-        for k in range(top)
+    mirror = place(across(z) * per_plane + p)
+
+    def to_mirror(src, dst, source_sem, target_sem):
+        return pltpu.make_async_remote_copy(
+            src_ref=src,
+            dst_ref=dst,
+            send_sem=source_sem,
+            recv_sem=target_sem,
+            device_id=mirror,
+            device_id_type=MESH,
+        )
+
+    routes = [
+        to_mirror(src, dst, far_send.at[i], far_recv.at[i])
+        for i, (src, dst) in enumerate(
+            ((ids, far_ids), (logits, far_logits), (weight, far_weight))
+        )
     ]
+    for route in routes:
+        route.start()
+
+    top = ids.shape[0]
+
+    def gate_columns(logit, group):
+        expo = jnp.exp(logit[...])
+        gates = group[...] * expo / jnp.sum(expo, axis=0, keepdims=True)
+        return [
+            jnp.transpose(jnp.broadcast_to(gates[k : k + 1], (rows, rows)))[:, :1]
+            for k in range(top)
+        ]
+
     before = (
         lax.broadcasted_iota(jnp.int32, (rows, rows), 0)
         < lax.broadcasted_iota(jnp.int32, (rows, rows), 1)
     ).astype(F32).astype(BF16)
-    id_rows = [ids[k : k + 1, :] for k in range(top)]
     rank_of = lax.broadcasted_iota(jnp.int32, (per_plane, cap, rows), 1).astype(F32)
 
-    def slots(plane):
+    def slots(plane, named_ids):
+        id_rows = [named_ids[k : k + 1, :] for k in range(top)]
         expert = lax.broadcasted_iota(jnp.int32, (per_plane, rows), 0) + plane * per_plane
         hits = [(row == expert).astype(F32) for row in id_rows]
         named = sum(hits)
@@ -275,98 +305,132 @@
             resid[:, c : c + tile] * scale * gain[:, c : c + tile]
         ).astype(BF16)
 
-    def group_copy(src, dst, g, i, source_sem, target_sem):
-        peer = (p + i) % per_plane
-        return pltpu.make_async_remote_copy(
-            src_ref=src.at[g, peer],
-            dst_ref=dst.at[g, p],
-            send_sem=source_sem.at[g],
-            recv_sem=target_sem.at[g],
-            device_id=place(flip(z, g) * per_plane + peer),
-            device_id_type=MESH,
-        )
-
-    def start_group(src, dst, g, source_sem, target_sem):
+    def start_group(src, dst, h, source_sem, target_sem):
         def one(i, carry):
-            @pl.when(g * per_plane + i > 0)
-            def _():
-                group_copy(src, dst, g, i, source_sem, target_sem).start()
-
+            peer = (p + i) % per_plane
+            pltpu.make_async_remote_copy(
+                src_ref=src.at[peer],
+                dst_ref=dst.at[p],
+                send_sem=source_sem,
+                recv_sem=target_sem,
+                device_id=place(near(z, h) * per_plane + peer),
+                device_id_type=MESH,
+            ).start()
             return carry
 
-        lax.fori_loop(0, per_plane, one, 0)
-
-    def wait_group(buf, g, sem):
-        @pl.when(g == 0)
-        def _():
-            part = buf.at[0, pl.ds(0, per_plane - 1)]
-            pltpu.make_async_copy(part, part, sem.at[0]).wait()
-
-        @pl.when(g > 0)
-        def _():
-            pltpu.make_async_copy(buf.at[g], buf.at[g], sem.at[g]).wait()
-
-    def dispatch(n, carry):
-        g = planes - 1 - n
-        named, hits, spread = slots(flip(z, g))
+        lax.fori_loop(1 - h, per_plane, one, 0)
+
+    def wait_group(buf, h, sem):
+        span = buf if h else buf.at[pl.ds(0, per_plane - 1)]
+        pltpu.make_async_copy(span, span, sem).wait()
+
+    def keep_in(q):
+        return pltpu.make_async_copy(send.at[2 * q, p], recv.at[2 * q, p], self_sem.at[q])
+
+    def keep_back(q, c):
+        return pltpu.make_async_copy(
+            outb.at[c, 2 * q, p], ret.at[c, 2 * q, p], self_back.at[PARTS * q + c]
+        )
+
+    tile = width // PARTS
+
+    def dispatch(q, h, source, named_ids):
+        g = 2 * q + h
+        named, hits, spread = slots(near(z, h), named_ids)
         pick = spread(named).astype(BF16)
         for c in range(0, width, tile):
             send[g, :, :, c : c + tile] = (
-                dot(pick, normed[:, c : c + tile])
+                dot(pick, source[:, c : c + tile])
                 .astype(BF16)
                 .reshape(per_plane, cap, tile)
             )
-        start_group(send, recv, g, out_sem, in_sem)
-        return carry
-
-    lax.fori_loop(0, planes, dispatch, 0)
-    keep = pltpu.make_async_copy(send.at[0, p], recv.at[0, p], self_sem)
-    keep.start()
-    keep.wait()
-    for load in loads[1:]:
-        load.wait()
-
-    def experts(g, carry):
-        wait_group(recv, g, in_sem)
-        x = recv[g].reshape(per_plane * cap, width)
+        start_group(send.at[g], recv.at[g], h, out_sem.at[g], in_sem.at[g])
+        if h == 0:
+            keep_in(q).start()
+
+    def experts(q, each):
+        keep_in(q).wait()
+        for h in range(2):
+            wait_group(recv.at[2 * q + h], h, in_sem.at[2 * q + h])
+        count = 2 * per_plane * cap
+        x = recv[2 * q : 2 * q + 2].reshape(count, width)
         ff = hidden.shape[1]
         for f in range(0, ff, 256):
             a = dot(x, wg[:, f : f + 256])
             b = dot(x, wu[:, f : f + 256])
             hidden[:, f : f + 256] = (a / (1.0 + jnp.exp(-a)) * b).astype(BF16)
-        h = hidden[...]
-        for c in range(0, width, tile):
-            outb[g, :, :, c : c + tile] = (
-                dot(h, wd[:, c : c + tile]).astype(BF16).reshape(per_plane, cap, tile)
+        for c in range(PARTS):
+            outb[c, 2 * q : 2 * q + 2] = (
+                dot(hidden[...], wd[:, c * tile : (c + 1) * tile])
+                .astype(BF16)
+                .reshape(2, per_plane, cap, tile)
             )
-        start_group(outb, ret, g, back_sem, home_sem)
-        return carry
-
-    lax.fori_loop(0, planes, experts, 0)
-    keep_back = pltpu.make_async_copy(outb.at[0, p], ret.at[0, p], self_sem)
-    keep_back.start()
-    keep_back.wait()
-
-    def combine(g, carry):
-        wait_group(ret, g, home_sem)
-        named, hits, spread = slots(flip(z, g))
-        picks = [jnp.transpose(spread(hit)).astype(BF16) for hit in hits]
-        for c in range(0, width, tile):
-            rows_in = ret[g, :, :, c : c + tile].reshape(per_plane * cap, tile)
-            resid[:, c : c + tile] += sum(
-                gate * dot(pick, rows_in) for gate, pick in zip(gate_cols, picks)
-            )
-        return carry
-
-    lax.fori_loop(0, planes, combine, 0)
-    out[...] = resid[...].astype(BF16)
-
-    def drain(g, carry):
-        wait_group(send, g, out_sem)
-        wait_group(outb, g, back_sem)
-        return carry
-
-    lax.fori_loop(0, planes, drain, 0)
+            each(q, c)
+
+    def give_back(q, c):
+        for h in (1, 0):
+            g, at = 2 * q + h, 4 * c + 2 * q + h
+            start_group(outb.at[c, g], ret.at[c, g], h, back_sem.at[at], home_sem.at[at])
+        keep_back(q, c).start()
+
+    def take_back(q, c):
+        keep_back(q, c).wait()
+        for h in range(2):
+            wait_group(ret.at[c, 2 * q + h], h, home_sem.at[4 * c + 2 * q + h])
+
+    def picks_of(named_ids):
+        spreads = [slots(near(z, h), named_ids) for h in range(2)]
+        return [
+            jnp.concatenate(
+                [jnp.transpose(spread(hits[k])) for _, hits, spread in spreads], axis=1
+            ).astype(BF16)
+            for k in range(top)
+        ]
+
+    def combined(q, c, picks, gates):
+        given = ret[c, 2 * q : 2 * q + 2].reshape(2 * per_plane * cap, tile)
+        return sum(gate * dot(pick, given) for gate, pick in zip(gates, picks))
+
+    dispatch(0, 1, normed, ids)
+    whole = to_mirror(normed, far, far_send.at[3], far_recv.at[3])
+    whole.start()
+    dispatch(0, 0, normed, ids)
+    for load in loads[1:]:
+        load.wait()
+    for route in routes:
+        route.wait()
+
+    experts(0, lambda q, c: None)
+    whole.wait()
+    dispatch(1, 1, far, far_ids)
+    dispatch(1, 0, far, far_ids)
+    for c in range(PARTS):
+        give_back(0, c)
+    far_picks, far_gates = picks_of(far_ids), gate_columns(far_logits, far_weight)
+    experts(1, give_back)
+
+    parts = [
+        to_mirror(halves.at[c], part_in.at[c], part_send.at[c], part_recv.at[c])
+        for c in range(PARTS)
+    ]
+    for c in range(PARTS):
+        take_back(1, c)
+        halves[c] = combined(1, c, far_picks, far_gates).astype(BF16)
+        parts[c].start()
+    picks, gates = picks_of(ids), gate_columns(logits, weight)
+    for c in range(PARTS):
+        take_back(0, c)
+        resid[:, c * tile : (c + 1) * tile] += combined(0, c, picks, gates)
+    for c in range(PARTS):
+        parts[c].wait()
+        out[:, c * tile : (c + 1) * tile] = (
+            resid[:, c * tile : (c + 1) * tile] + part_in[c].astype(F32)
+        ).astype(BF16)
+
+    for g in range(4):
+        wait_group(send.at[g], g % 2, out_sem.at[g])
+        for c in range(PARTS):
+            wait_group(outb.at[c, g], g % 2, back_sem.at[4 * c + g])
 
 
 def fused(
@@ -380,7 +444,9 @@
     top = route_ids.shape[1]
     vmem = pl.BlockSpec(memory_space=pltpu.VMEM)
     anywhere = pl.BlockSpec(memory_space=pl.ANY)
-    blocks = pltpu.VMEM((planes, per_plane, cap, width), BF16)
+    blocks = pltpu.VMEM((4, per_plane, cap, width), BF16)
+    cut = pltpu.VMEM((PARTS, 4, per_plane, cap, width // PARTS), BF16)
+    slab = pltpu.VMEM((PARTS, rows, width // PARTS), BF16)
     dma = pltpu.SemaphoreType.DMA
     return pl.pallas_call(
         functools.partial(fused_kernel, tp_size, planes, per_plane, cap),
@@ -399,10 +465,16 @@
             pltpu.VMEM((rows, chan), BF16),
             pltpu.VMEM((rows, width), F32),
             pltpu.VMEM((rows, width), BF16),
-            pltpu.VMEM((per_plane * cap, ff), BF16),
-            blocks, blocks, blocks, blocks,
-            dma((4,)), dma((4,)), dma((4,)), dma, dma, dma,
-            dma((planes,)), dma((planes,)), dma((planes,)), dma((planes,)),
+            pltpu.VMEM((2 * per_plane * cap, ff), BF16),
+            blocks, blocks, cut, cut,
+            pltpu.VMEM((rows, width), BF16),
+            pltpu.VMEM((top, rows), jnp.int32),
+            pltpu.VMEM((top, rows), F32),
+            pltpu.VMEM((1, rows), F32),
+            slab, slab,
+            dma((4,)), dma((4,)), dma((4,)), dma, dma, dma((2,)), dma((2 * PARTS,)),
+            dma((4,)), dma((4,)), dma((4 * PARTS,)), dma((4 * PARTS,)),
+            dma((4,)), dma((4,)), dma((PARTS,)), dma((PARTS,)),
         ],
         compiler_params=pltpu.CompilerParams(
             collective_id=0, has_side_effects=True, vmem_limit_bytes=56 * 1024 * 1024

time: 111 us -> 99.1 us (0.89)
  the two profiles are of different devices: /device:TPU:19 before, /device:TPU:0 now
where the time goes in v2:
time: 99.1 us; the launch traced here: 98.9 us
  Pallas kernels  97 us (98%)
  local copies, waits for them, and re-layouts  1.88 us (2%)
    pallas_call x1, Pallas kernels, fused(): pl.pallas_call(functools.partial(fused_kernel, tp_size, planes, per_plane...  97 us

profile of v2, /device:TPU:0, one launch (start us, length us, event | category | flops | bytes accessed | tf_op | source)
XLA Modules:
  0.0 98.9 jit_solution(10695729297655493609)
XLA Ops:
  0.0 97.0 %shard_map.136 = bf16[128,2048]{1,0:T(8,128)(2,1)} custom-call(bf16[128,2048]{1,0:T(8,128)(2,1)} %stream.1, bf16[256,512]{1,0:T(8,128)(2,1)} %outer.1, bf16[256,512]{1,0:T(8,128)(2,1)} %inner.1, bf16[256,512]{1,0:T(8,128)(2,1)} %values.1, s32[1,256]{1,0:T(1,128)} %bitcast.6, f32[3,512]{1,0:T(4,128)} %taps.1, f32[1,2048]{1,0:T(1,128)} %bitcast.5, ...), custom_call_target="tpu_custom_call" | custom-call | tf_op jit(solution)/shard_map/pallas_call | solution.py:451
  97.0 1.9 %copy.16 = bf16[128,2048]{1,0:T(8,128)(2,1)} copy(bf16[128,2048]{1,0:T(8,128)(2,1)} %shard_map.136) | data formatting | bytes 1048576

commit v3 on v2

--- a/solution.py
+++ b/solution.py
@@ -404,10 +404,10 @@
     whole.wait()
     dispatch(1, 1, far, far_ids)
     dispatch(1, 0, far, far_ids)
+    far_picks, far_gates = picks_of(far_ids), gate_columns(far_logits, far_weight)
+    experts(1, give_back)
     for c in range(PARTS):
         give_back(0, c)
-    far_picks, far_gates = picks_of(far_ids), gate_columns(far_logits, far_weight)
-    experts(1, give_back)
 
     parts = [
         to_mirror(halves.at[c], part_in.at[c], part_send.at[c], part_recv.at[c])

time: 99.1 us -> 98.4 us (level)
  no operation moved by 1% of the time
where the time goes in v3:
time: 98.4 us; the launch traced here: 98.2 us
  Pallas kernels  96.3 us (98%)
  local copies, waits for them, and re-layouts  1.88 us (2%)
    pallas_call x1, Pallas kernels, fused(): pl.pallas_call(functools.partial(fused_kernel, tp_size, planes, per_plane...  96.3 us

profile of v3, /device:TPU:0, one launch (start us, length us, event | category | flops | bytes accessed | tf_op | source)
XLA Modules:
  0.0 98.2 jit_solution(1742452054245557336)
XLA Ops:
  0.0 96.3 %shard_map.136 = bf16[128,2048]{1,0:T(8,128)(2,1)} custom-call(bf16[128,2048]{1,0:T(8,128)(2,1)} %stream.1, bf16[256,512]{1,0:T(8,128)(2,1)} %outer.1, bf16[256,512]{1,0:T(8,128)(2,1)} %inner.1, bf16[256,512]{1,0:T(8,128)(2,1)} %values.1, s32[1,256]{1,0:T(1,128)} %bitcast.6, f32[3,512]{1,0:T(4,128)} %taps.1, f32[1,2048]{1,0:T(1,128)} %bitcast.5, ...), custom_call_target="tpu_custom_call" | custom-call | tf_op jit(solution)/shard_map/pallas_call | solution.py:451
  96.3 1.9 %copy.16 = bf16[128,2048]{1,0:T(8,128)(2,1)} copy(bf16[128,2048]{1,0:T(8,128)(2,1)} %shard_map.136) | data formatting | bytes 1048576
